TPU v7x, 128 devices: a whole 4x4x4 slice. The times are simulated.
128 devices in a mesh: sp: 32 (over z, y, core), tp: 4 (over x).
Axes of the slice: x: 4, y: 4, z: 4, core: 2. Of those that a mesh axis runs over, the one named last changes fastest.
Arguments:
- queries: bfloat16 [16384, 1024], P('sp', 'tp'), may hold values from -6 to 6
- keys: bfloat16 [16384, 1024], P('sp', 'tp'), may hold values from -6 to 6
- values: bfloat16 [16384, 1024], P('sp', 'tp'), may hold values from -6 to 6
- cum_gate: float32 [16384, 16], P('sp', 'tp'), as said below
- documents: int32 [16384], P('sp'), may hold values from 0 to 3, never falling along the last dimension, each value on 1 to 8192 neighbouring positions
- head_gain: float32 [1024], P('tp'), may hold values from 0.1 to 1.9
- out_weight: bfloat16 [1024, 2048], replicated, may hold values from -0.1875 to 0.1875
- resid: bfloat16 [16384, 2048], P(('sp', 'tp')), may hold values from -6 to 6
- norm_gain: float32 [2048], replicated, may hold values from 0.1 to 1.9
- routes: int32 [16384, 2], P(('sp', 'tp')), may hold values from 0 to 31, all different within a row; in each aligned block of 128 rows (0 to 127, 128 to 255, ...) at most 16 rows name the same one
- route_weights: float32 [16384, 2], P(('sp', 'tp')), may hold values from 0.25 to 1
- w_gate: bfloat16 [32, 2048, 3584], P('sp', None, 'tp'), may hold values from -0.125 to 0.125
- w_up: bfloat16 [32, 2048, 3584], P('sp', None, 'tp'), may hold values from -0.125 to 0.125
- w_down: bfloat16 [32, 3584, 2048], P('sp', 'tp'), may hold values from -0.09375 to 0.09375
Outputs:
- mixed: bfloat16 [16384, 2048], P(('sp', 'tp'))
Inputs may be any that keep to these rules, and one draw needn't show every extreme that they name: `cum_gate`: along the positions each head's values never rise. `documents`: document numbers never fall along the positions. `routes`: the 2 experts of a row differ. In each aligned block of 128 rows no expert is named more than 16 times; in some blocks an expert is named exactly 16 times.
All inputs are finite; a program needn't handle non-finite values.
Results may differ from a plain program's by a relative error of at most 0.015.
Values may be sent and summed in bfloat16 or wider, within the bound.
A program may use at most 128 MiB of HBM per device.

v0:
```python
import jax
import jax.numpy as jnp
from jax import lax
from jax.experimental import pallas as pl
from jax.experimental.pallas import tpu as pltpu
from jax.sharding import PartitionSpec as P

EPS = 1e-06
LOG2E = 1.4426950408889634
BLK = 512
EXTRA = 32
NEG = -1e30
F32 = jnp.float32
BF16 = jnp.bfloat16


def pieces_of(x):
    hi = lax.reduce_precision(x, 8, 7)
    rest = x - hi
    mid = lax.reduce_precision(rest, 8, 7)
    return hi, mid, rest - mid


def attention_kernel(q_ref, kvx_ref, gain_ref, o_ref, kp, vt, qp, acc, mrow, g0):
    members = kvx_ref.shape[0]
    groups = kvx_ref.shape[1]
    blocks = members * groups
    me = lax.rem(lax.axis_index("sp"), members)
    lane = lax.broadcasted_iota(jnp.int32, (128, 128), 1)
    lane_wide = lax.broadcasted_iota(jnp.int32, (BLK, 128), 1)
    row_extra = lax.broadcasted_iota(jnp.int32, (EXTRA, 128), 0)
    is_doc = (row_extra >= 12) & (row_extra < 16)

    def prepare(kb, counts):
        member, group = lax.rem(kb, members), kb // members
        extra = kvx_ref[member, group, BLK : BLK + EXTRA, :].astype(F32)
        g0[kb] = jnp.sum(jnp.where(row_extra == 16, extra, 0.0))
        counts = tuple(
            count + jnp.where(is_doc & (extra < d + 0.5), 1.0, 0.0)
            for d, count in enumerate(counts)
        )
        turned = jnp.concatenate([extra, jnp.zeros((128 - EXTRA, 128), F32)], axis=0).T
        for c in range(4):
            kp[kb, c * 128 : (c + 1) * 128, 128:256] = jnp.where(
                (lane < 12) & (lane % 4 == c), turned, 0.0
            ).astype(BF16)
        kv = kvx_ref[member, group, 0:BLK, :].astype(F32)
        kp[kb, :, 0:128] = jnp.where(lane_wide < 64, kv, pltpu.roll(kv, 64, 1)).astype(BF16)
        vt[kb, 16:80, :] = kv.T[64:128, :].astype(BF16)
        vt[kb, 0:16, :] = jnp.ones((16, BLK), BF16)
        return counts

    zero = jnp.zeros((EXTRA, 128), F32)
    counts = lax.fori_loop(0, blocks, prepare, (zero, zero, zero))
    starts = [jnp.sum(c).astype(jnp.int32) for c in counts]

    def one_query_block(i, unused):
        qb = i * members + me
        half = q_ref[i].astype(F32) * (LOG2E * 0.125)
        q = jnp.concatenate([half, pltpu.roll(half, 64, 1)], axis=0)
        hi = q.astype(BF16).astype(F32)
        low = pltpu.roll(q - hi, 64, 1)
        qp[:, 0:128] = jnp.where(lane_wide < 64, hi, low).astype(BF16)
        qp[:, 128:256] = jnp.where(lane_wide < 12, 1.0, 0.0).astype(BF16)
        extra = kvx_ref[me, i, BLK : BLK + EXTRA, :].astype(F32)
        doc = jnp.concatenate([extra[12 + c : 13 + c, :] for c in range(4)], axis=1)
        start = jnp.where(
            doc < 0.5,
            0,
            jnp.where(doc < 1.5, starts[0], jnp.where(doc < 2.5, starts[1], starts[2])),
        )
        first = jnp.min(start)
        last = jnp.max(start)
        base = g0[qb]

        def visit(kb, masked, fresh):
            shift = (base - g0[kb]) * LOG2E
            scores = lax.dot_general(
                kp[kb], qp[...], (((1,), (1,)), ((), ())), preferred_element_type=F32
            )
            if masked:
                key_pos = kb * BLK + lax.broadcasted_iota(jnp.int32, (BLK, BLK), 0)
                query_pos = qb * BLK + lax.broadcasted_iota(jnp.int32, (BLK, BLK), 1)
                allowed = (key_pos <= query_pos) & (key_pos >= start)
                scores = jnp.where(allowed, scores, NEG)
            top = jnp.max(scores, axis=0, keepdims=True) + shift
            if not fresh:
                old = mrow[...]
                top = jnp.maximum(old, top)
            weights = jnp.exp2(scores - (top - shift)).astype(BF16)
            added = jnp.dot(vt[kb], weights, preferred_element_type=F32)
            if fresh:
                acc[...] = added
            else:
                acc[...] = acc[...] * jnp.exp2(old - top) + added
            mrow[...] = top

        visit(qb, True, True)

        def earlier(kb, carry):
            plain = kb * BLK >= last

            @pl.when(plain)
            def _():
                visit(kb, False, False)

            @pl.when(jnp.logical_not(plain))
            def _():
                visit(kb, True, False)

            return carry

        lax.fori_loop(first // BLK, qb, earlier, 0)
        out = acc[16:80, :] / acc[0:1, :]
        mean_square = jnp.mean(out * out, axis=0, keepdims=True)
        gain = jnp.concatenate([gain_ref[...]] * 4, axis=1)
        o_ref[i] = (out * lax.rsqrt(mean_square + EPS) * gain).astype(BF16)
        return unused

    lax.fori_loop(0, groups, one_query_block, 0)


def attend(q, kvx, gain):
    members, groups = kvx.shape[:2]
    blocks = members * groups
    vmem = pl.BlockSpec(memory_space=pltpu.VMEM)
    return pl.pallas_call(
        attention_kernel,
        out_shape=jax.ShapeDtypeStruct((groups, 64, BLK), BF16),
        in_specs=[vmem] * 3,
        out_specs=vmem,
        scratch_shapes=[
            pltpu.VMEM((blocks, BLK, 256), BF16),
            pltpu.VMEM((blocks, 80, BLK), BF16),
            pltpu.VMEM((BLK, 256), BF16),
            pltpu.VMEM((80, BLK), F32),
            pltpu.VMEM((1, BLK), F32),
            pltpu.SMEM((blocks,), F32),
        ],
        compiler_params=pltpu.CompilerParams(vmem_limit_bytes=48 * 1024 * 1024),
        name="attention",
    )(q, kvx, gain)


MESH = pl.DeviceIdType.MESH
GROUP = 4


def experts_kernel(
    out_ref, wg_hbm, wu_hbm, wd_hbm, ret_ref,
    x, p, r_in, m_in, wg, wu, wd,
    w_sem, a2a_send, a2a_recv, ag_send, ag_recv, relay_send, relay_recv,
    r_send, r_recv, m_send, m_recv, ret_send, ret_recv,
):
    experts, slots, width = out_ref.shape
    tps = x.shape[0]
    steps = experts // GROUP
    half = GROUP // 2
    s = lax.axis_index("sp")
    t = lax.axis_index("tp")
    right = lax.rem(t + 1, tps)
    left = lax.rem(t + tps - 1, tps)
    far = lax.rem(t + 2, tps)
    sides = (right, left)

    loads = [
        pltpu.make_async_copy(a.at[0], b, w_sem.at[i])
        for i, (a, b) in enumerate(((wg_hbm, wg), (wu_hbm, wu), (wd_hbm, wd)))
    ]
    for load in loads:
        load.start()

    barrier = pltpu.get_barrier_semaphore()

    @pl.loop(1, experts)
    def _(k):
        pl.semaphore_signal(
            barrier, 1, device_id=(lax.rem(s + k, experts), t), device_id_type=MESH
        )

    for side in sides:
        pl.semaphore_signal(barrier, 1, device_id=(s, side), device_id_type=MESH)
    pl.semaphore_wait(barrier, experts - 1 + 2)

    def send(src, dst, send_sem, recv_sem, sp, tp):
        return pltpu.make_async_remote_copy(
            src_ref=src,
            dst_ref=dst,
            send_sem=send_sem,
            recv_sem=recv_sem,
            device_id=(sp, tp),
            device_id_type=MESH,
        )

    def to_side(i, src, dst, send_sem, recv_sem):
        return send(src, dst, send_sem, recv_sem, s, sides[i])

    @pl.loop(1, experts)
    def _(k):
        to = lax.rem(s + k, experts)
        send(out_ref.at[to], x.at[t, k], a2a_send, a2a_recv.at[k // GROUP], to, t).start()

    x[t, 0] = out_ref[s]

    def whole(c):
        return pl.ds(c * GROUP, GROUP)

    def part(c, i):
        return pl.ds(c * GROUP + i * half, half)

    def enter(c):
        @pl.when(c == 0)
        def _():
            first = x.at[t, pl.ds(1, GROUP - 1)]
            send(first, first, a2a_send, a2a_recv.at[0], s, right).wait_recv()

        @pl.when(c > 0)
        def _():
            rows = x.at[t, whole(c)]
            send(rows, rows, a2a_send, a2a_recv.at[c], s, right).wait_recv()

        rows = x.at[t, whole(c)]
        for i in range(2):
            to_side(i, rows, rows, ag_send.at[i], ag_recv.at[i, c]).start()

    def relay(c):
        for i in range(2):
            origin = sides[1 - i]
            rows = x.at[origin, whole(c)]
            to_side(i, rows, rows, ag_send.at[i], ag_recv.at[i, c]).wait_recv()
            rows = x.at[origin, part(c, i)]
            to_side(i, rows, rows, relay_send.at[i], relay_recv.at[i, c]).start()

    def compute(c):
        for i in range(2):
            rows = x.at[far, part(c, i)]
            to_side(i, rows, rows, relay_send.at[i], relay_recv.at[i, c]).wait_recv()
        rows = x[:, whole(c)].reshape(tps * GROUP * slots, width)
        gate = jnp.dot(rows, wg[...], preferred_element_type=F32)
        up = jnp.dot(rows, wu[...], preferred_element_type=F32)
        hidden = (gate / (1.0 + jnp.exp(-gate)) * up).astype(BF16)
        made = jnp.dot(hidden, wd[...], preferred_element_type=F32)
        p[:, whole(c)] = made.astype(BF16).reshape(tps, GROUP, slots, width)
        for i in range(2):
            to_side(
                i, p.at[far, part(c, i)], r_in.at[i, pl.ds(c * half, half)],
                r_send.at[i], r_recv.at[i, c],
            ).start()

    def pass_on(c):
        for i in range(2):
            got = r_in.at[i, pl.ds(c * half, half)]
            to_side(i, got, got, r_send.at[i], r_recv.at[i, c]).wait_recv()
            mine = p[sides[i], part(c, i)].astype(F32)
            p[sides[i], part(c, i)] = (mine + got[...].astype(F32)).astype(BF16)
        for i in range(2):
            to_side(
                i, p.at[sides[i], whole(c)], m_in.at[i, whole(c)], m_send.at[i], m_recv.at[i, c]
            ).start()

    def leave(c):
        total = p[t, whole(c)].astype(F32)
        for i in range(2):
            got = m_in.at[i, whole(c)]
            to_side(i, got, got, m_send.at[i], m_recv.at[i, c]).wait_recv()
            total = total + got[...].astype(F32)
        p[t, whole(c)] = total.astype(BF16)

        @pl.when(c == 0)
        def _():
            ret_ref[s] = p[t, 0]

        @pl.loop(jnp.where(c == 0, 1, 0), GROUP)
        def _(j):
            k = c * GROUP + j
            to = lax.rem(s + experts - k, experts)
            send(p.at[t, k], ret_ref.at[s], ret_send, ret_recv, to, t).start()

    @pl.loop(0, steps + 4)
    def _(i):
        @pl.when(i < steps)
        def _():
            enter(i)

        @pl.when((i >= 1) & (i < steps + 1))
        def _():
            relay(i - 1)

        @pl.when(i >= 4)
        def _():
            leave(i - 4)

        @pl.when((i >= 3) & (i < steps + 3))
        def _():
            pass_on(i - 3)

        @pl.when(i == 2)
        def _():
            for load in loads:
                load.wait()

        @pl.when((i >= 2) & (i < steps + 2))
        def _():
            compute(i - 2)

    most = x.at[0, pl.ds(0, experts - 1)]
    every = x.at[0]
    some = x.at[0, pl.ds(0, experts // 2)]
    back = ret_ref.at[pl.ds(0, experts - 1)]
    send(most, back, a2a_send, ret_recv, s, right).wait_send()
    send(most, back, ret_send, ret_recv, s, right).wait()
    for i in range(2):
        to_side(i, every, every, ag_send.at[i], ag_recv.at[i, 0]).wait_send()
        to_side(i, some, some, relay_send.at[i], relay_recv.at[i, 0]).wait_send()
        to_side(i, some, some, r_send.at[i], r_recv.at[i, 0]).wait_send()
        to_side(i, every, every, m_send.at[i], m_recv.at[i, 0]).wait_send()


def at_experts(outbound, w_gate, w_up, w_down):
    experts, slots, width = outbound.shape
    hidden = w_gate.shape[2]
    tps = lax.axis_size("tp")
    steps = experts // GROUP
    vmem = pl.BlockSpec(memory_space=pltpu.VMEM)
    hbm = pl.BlockSpec(memory_space=pl.ANY)
    dma = pltpu.SemaphoreType.DMA
    return pl.pallas_call(
        experts_kernel,
        out_shape=jax.ShapeDtypeStruct(outbound.shape, BF16),
        in_specs=[vmem, hbm, hbm, hbm],
        out_specs=vmem,
        scratch_shapes=[
            pltpu.VMEM((tps, experts, slots, width), BF16),
            pltpu.VMEM((tps, experts, slots, width), BF16),
            pltpu.VMEM((2, experts // 2, slots, width), BF16),
            pltpu.VMEM((2, experts, slots, width), BF16),
            pltpu.VMEM((width, hidden), BF16),
            pltpu.VMEM((width, hidden), BF16),
            pltpu.VMEM((hidden, width), BF16),
            dma((3,)),
            dma,
            dma((steps,)),
            dma((2,)),
            dma((2, steps)),
            dma((2,)),
            dma((2, steps)),
            dma((2,)),
            dma((2, steps)),
            dma((2,)),
            dma((2, steps)),
            dma,
            dma,
        ],
        compiler_params=pltpu.CompilerParams(
            collective_id=1, has_side_effects=True, vmem_limit_bytes=58 * 1024 * 1024
        ),
        name="experts",
    )(outbound, w_gate, w_up, w_down)


def on_device(
    queries,
    keys,
    values,
    cum_gate,
    documents,
    head_gain,
    out_weight,
    resid,
    norm_gain,
    routes,
    route_weights,
    w_gate,
    w_up,
    w_down,
):
    tokens = queries.shape[0]
    heads = cum_gate.shape[1]
    sp_count = lax.axis_size("sp")
    members = sp_count // heads
    z = lax.axis_index("sp") // members

    def by_head(a):
        return a.reshape(tokens, heads, 64).transpose(1, 0, 2)

    qh = by_head(queries)
    q_pack = jnp.concatenate([qh[:, : BLK // 2], qh[:, BLK // 2 :]], axis=-1)
    kv = jnp.concatenate([by_head(keys), by_head(values)], axis=-1)
    gate = cum_gate.T
    gate0 = gate[:, :1]
    rel = jnp.stack(pieces_of((gate0 - gate) * LOG2E), axis=1).reshape(heads, 12, 128)
    docs = jnp.broadcast_to(documents.astype(F32).reshape(1, 4, 128), (heads, 4, 128))
    zero_row = jnp.pad(jnp.stack(pieces_of(gate0), axis=2), ((0, 0), (0, 15), (0, 125)))
    extra = jnp.concatenate([rel, docs, zero_row], axis=1).astype(BF16)
    payload = jnp.concatenate([kv, extra, q_pack], axis=1)
    columns = [[j + members * g for g in range(heads)] for j in range(members)]
    rows = [[j + members * g for j in range(members)] for g in range(heads)]
    arrived = lax.all_to_all(
        payload, "sp", split_axis=0, concat_axis=0, axis_index_groups=columns, tiled=True
    )
    kvx = lax.all_gather(arrived[:, : BLK + EXTRA], "sp", axis=0, axis_index_groups=rows)
    gain = jnp.broadcast_to(lax.dynamic_slice_in_dim(head_gain, z * 64, 64)[:, None], (64, 128))
    normed = attend(arrived[:, BLK + EXTRA :], kvx, gain)
    normed = lax.all_to_all(
        normed, "sp", split_axis=0, concat_axis=0, axis_index_groups=columns, tiled=True
    ).reshape(heads * 64, tokens)
    tp_count = lax.axis_size("tp")
    local_rows = tokens // tp_count
    regrouped = lax.all_to_all(normed, "tp", split_axis=1, concat_axis=0, tiled=True)
    projected = lax.dot_general(
        regrouped, out_weight, (((0,), (0,)), ((), ())), preferred_element_type=F32
    )
    stream = lax.optimization_barrier((resid.astype(F32) + projected).astype(BF16))
    widened = stream.astype(F32)
    mean_wide = jnp.mean(widened * widened, axis=-1, keepdims=True)
    expert_input = (widened * lax.rsqrt(mean_wide + EPS) * norm_gain).astype(BF16)
    top_count = routes.shape[1]
    expert_count = sp_count
    model_width = stream.shape[1]
    capacity = 2 * top_count * tokens // (tp_count * expert_count)
    flat_routes = routes.reshape(-1)
    route_total = flat_routes.shape[0]
    onehot = (flat_routes[:, None] == jnp.arange(expert_count, dtype=jnp.int32)[None, :]).astype(
        jnp.int32
    )
    ranks = jnp.sum(jnp.cumsum(onehot, axis=0) * onehot, axis=1) - 1
    targets = flat_routes * capacity + ranks
    owners = jnp.arange(route_total, dtype=jnp.int32) // top_count
    slot_owner = jnp.zeros((expert_count * capacity,), jnp.int32).at[targets].set(owners)
    slot_used = jnp.zeros((expert_count * capacity,), jnp.bool_).at[targets].set(True)
    outbound = jnp.where(slot_used[:, None], expert_input[slot_owner], jnp.zeros((), BF16))
    outbound = outbound.reshape(expert_count, capacity, model_width)

    returned = at_experts(outbound, w_gate, w_up, w_down)
    results = returned.reshape(expert_count * capacity, model_width)[targets]
    results = results.reshape(local_rows, top_count, model_width)
    mixed = widened + jnp.sum(route_weights[:, :, None] * results.astype(F32), axis=1)
    return mixed.astype(BF16)


def solution(mesh):
    in_specs = (
        P("sp", "tp"),
        P("sp", "tp"),
        P("sp", "tp"),
        P("sp", "tp"),
        P("sp"),
        P("tp"),
        P(),
        P(("sp", "tp"), None),
        P(),
        P(("sp", "tp"), None),
        P(("sp", "tp"), None),
        P("sp", None, "tp"),
        P("sp", None, "tp"),
        P("sp", "tp", None),
    )
    out_specs = P(("sp", "tp"), None)
    return jax.shard_map(
        on_device, mesh=mesh, in_specs=in_specs, out_specs=out_specs, check_vma=False
    )
```

profile of v0, /device:TPU:1, one launch (start us, length us, event | category | flops | bytes accessed | tf_op | source)
XLA Modules:
  0.0 308.8 jit_solution(9436732705010422351)
XLA Ops:
  6.5 0.9 slice_reduce_fusion.1
  7.4 0.8 fusion.23
  8.2 1.1 copy.38
  9.3 0.3 copy.39
  9.6 1.1 copy.36
  10.7 0.3 copy.37
  11.5 0.3 copy.45
  11.9 0.3 pad_maximum_fusion
  12.4 0.3 concatenate.14
  12.8 17.1 %all_to_all.29 = bf16[4,800,128]{2,1,0:T(8,128)(2,1)S(1)} all-to-all(bf16[4,800,128]{2,1,0:T(8,128)(2,1)S(1)} %concatenate.14), channel_id=1, replica_groups={{0,32,64,96},{4,36,68,100},{8,40,72,104},{12,44,76,108},{16,48,80,112},..., dimensions={0} | all-to-all | bytes 1638400 | tf_op jit(solution)/shard_map/all_to_all | solution.py:398
  29.9 0.8 slice.36
  31.5 0.6 reduce-window.6
  32.5 1.4 scatter_custom_fusion.1
  33.9 1.5 scatter_custom_fusion
  35.7 29.8 %all-gather.3.cloned.1.call-done = bf16[32,544,128]{2,1,0:T(8,128)(2,1)} async-done(((bf16[4,544,128]{2,1,0:T(8,128)(2,1)}), bf16[32,544,128]{2,1,0:T(8,128)(2,1)}) %all-gather.3.cloned.1.call-update) | async-done | bytes 4456464 | tf_op jit(solution)/shard_map/all_gather | solution.py:401
  65.5 2.3 copy-done
  67.8 29.8 %attention.1 = bf16[4,64,512]{2,1,0:T(8,128)(2,1)} custom-call(bf16[4,256,128]{2,1,0:T(8,128)(2,1)S(1)} %slice.35.q_ref, bf16[8,4,544,128]{3,2,1,0:T(8,128)(2,1)S(1)} %bitcast.43, f32[64,128]{1,0:T(8,128)S(1)} %broadcast_in_dim.46.gain_ref), custom_call_target="tpu_custom_call" | custom-call | tf_op jit(solution)/shard_map/attention/pallas_call | solution.py:127
  97.6 4.3 %all-to-all-start.1 = ((bf16[4,64,512]{2,1,0:T(8,128)(2,1)}), bf16[4,64,512]{2,1,0:T(8,128)(2,1)S(1)}, u32[]{:S(2)}, u32[]{:S(2)}) async-start(bf16[4,64,512]{2,1,0:T(8,128)(2,1)} %attention.1), calls=%async_computation.1 | async-start | bytes 524288 | tf_op jit(solution)/shard_map/all_to_all | solution.py:404
  101.8 5.5 %all-to-all-done.1 = bf16[4,64,512]{2,1,0:T(8,128)(2,1)S(1)} async-done(((bf16[4,64,512]{2,1,0:T(8,128)(2,1)}), bf16[4,64,512]{2,1,0:T(8,128)(2,1)S(1)}, u32[]{:S(2)}, u32[]{:S(2)}) %all-to-all-start.1) | async-done | bytes 262176 | tf_op jit(solution)/shard_map/all_to_all | solution.py:404
  107.4 0.7 copy.46
  108.2 4.0 %all-to-all-start.2 = ((bf16[256,4,128]{2,0,1:T(8,128)(2,1)}), bf16[256,4,128]{2,0,1:T(8,128)(2,1)S(1)}, u32[]{:S(2)}, u32[]{:S(2)}) async-start(bf16[256,4,128]{2,0,1:T(8,128)(2,1)} %copy.46), calls=%async_computation.2 | async-start | bytes 524288 | tf_op jit(solution)/shard_map/all_to_all | solution.py:409
  112.2 6.9 %all-to-all-done.2 = bf16[256,4,128]{2,0,1:T(8,128)(2,1)S(1)} async-done(((bf16[256,4,128]{2,0,1:T(8,128)(2,1)}), bf16[256,4,128]{2,0,1:T(8,128)(2,1)S(1)}, u32[]{:S(2)}, u32[]{:S(2)}) %all-to-all-start.2) | async-done | bytes 262176 | tf_op jit(solution)/shard_map/all_to_all | solution.py:409
  119.1 2.9 fusion
  122.0 0.2 fusion.1
  122.2 0.2 fusion.3
  122.4 2.5 gather_fusion
  124.9 1.5 broadcast_select_fusion.out_ref
  126.4 163.9 %experts.1 = bf16[32,16,2048]{2,1,0:T(8,128)(2,1)} custom-call(bf16[32,16,2048]{2,1,0:T(8,128)(2,1)} %broadcast_select_fusion.out_ref, bf16[1,2048,896]{2,1,0:T(8,128)(2,1)} %wg_hbm.1, bf16[1,2048,896]{2,1,0:T(8,128)(2,1)} %wu_hbm.1, bf16[1,896,2048]{2,1,0:T(8,128)(2,1)} %wd_hbm.1), custom_call_target="tpu_custom_call" | custom-call | tf_op jit(solution)/shard_map/experts/pallas_call | solution.py:327
  290.3 5.2 %gather_fusion.1 = bf16[256,2048]{1,0:T(8,128)(2,1)} fusion(bf16[512,2048]{1,0:T(8,128)(2,1)} %bitcast.44, s32[1024]{0:T(1024)S(1)} %pad_clamp_fusion), kind=kCustom, calls=%fused_computation.1 | custom fusion | bytes 2098176 | tf_op jit(solution)/shard_map/gather | solution.py:435
  295.5 2.4 reshape.103
  297.9 3.2 %multiply_reduce_fusion = f32[128,2048]{1,0:T(8,128)S(1)} fusion(f32[128,2,2048]{2,1,0:T(2,128)S(1)} %reshape.103, f32[128,2]{1,0:T(8,128)S(1)} %copy.47), kind=kLoop, calls=%fused_computation.6 | loop fusion | flops 786432 | bytes 3146752 | tf_op jit(solution)/shard_map/reduce_sum | solution.py:437
  301.0 0.9 fusion.4
  (57 shorter events, 2.3 us)
Async XLA Ops:
  6.5 4.5 %copy-start.3 = (f32[512,4]{0,1:T(4,128)S(1)}, f32[512,4]{0,1:T(4,128)}, u32[]{:S(2)}) copy-start(f32[512,4]{0,1:T(4,128)} %param.17) | copy-start | bytes 24580
  6.5 4.6 %copy-start.6 = (s32[512]{0:T(512)S(1)}, s32[512]{0:T(512)}, u32[]{:S(2)}) copy-start(s32[512]{0:T(512)} %param.18) | copy-start | bytes 6148
  6.5 4.9 %copy-start.2 = (bf16[512,256]{1,0:T(8,128)(2,1)S(1)}, bf16[512,256]{1,0:T(8,128)(2,1)}, u32[]{:S(2)}) copy-start(bf16[512,256]{1,0:T(8,128)(2,1)} %param.14) | copy-start | bytes 786436
  6.5 58.9 %all-gather.3.cloned.1.call-start = ((), (), s32[]{:S(2)}) async-start(), calls=%async_computation.3 | async-start | bytes 5013504 | tf_op jit(solution)/shard_map/all_gather | solution.py:401
  12.4 18.4 %copy-start.5 = (s32[128,2]{0,1:T(2,128)S(1)}, s32[128,2]{0,1:T(2,128)}, u32[]{:S(2)}) copy-start(s32[128,2]{0,1:T(2,128)} %param.23) | copy-start | bytes 3076
  12.8 22.7 %copy-start.7 = (f32[128,2]{0,1:T(2,128)S(1)}, f32[128,2]{0,1:T(2,128)}, u32[]{:S(2)}) copy-start(f32[128,2]{0,1:T(2,128)} %param.24) | copy-start | bytes 3076
  12.8 22.8 %copy-start.8 = (f32[256]{0:T(256)S(1)}, f32[256]{0:T(256)}, u32[]{:S(2)}) copy-start(f32[256]{0:T(256)} %param.19) | copy-start | bytes 3076
  65.5 2.3 copy-start
  97.6 21.5 %copy-start.1 = (bf16[128,2048]{1,0:T(8,128)(2,1)S(1)}, bf16[128,2048]{1,0:T(8,128)(2,1)}, u32[]{:S(2)}) copy-start(bf16[128,2048]{1,0:T(8,128)(2,1)} %param.21) | copy-start | bytes 1572868
  97.6 9.8 %all-to-all-start.1 = ((bf16[4,64,512]{2,1,0:T(8,128)(2,1)}), bf16[4,64,512]{2,1,0:T(8,128)(2,1)S(1)}, u32[]{:S(2)}, u32[]{:S(2)}) async-start(bf16[4,64,512]{2,1,0:T(8,128)(2,1)} %attention.1), calls=%async_computation.1 | async-start | bytes 524288 | tf_op jit(solution)/shard_map/all_to_all | solution.py:404
  108.2 10.9 %all-to-all-start.2 = ((bf16[256,4,128]{2,0,1:T(8,128)(2,1)}), bf16[256,4,128]{2,0,1:T(8,128)(2,1)S(1)}, u32[]{:S(2)}, u32[]{:S(2)}) async-start(bf16[256,4,128]{2,0,1:T(8,128)(2,1)} %copy.46), calls=%async_computation.2 | async-start | bytes 524288 | tf_op jit(solution)/shard_map/all_to_all | solution.py:409
  119.1 3.2 %copy-start.4 = (f32[2048]{0:T(1024)S(1)}, f32[2048]{0:T(1024)}, u32[]{:S(2)}) copy-start(f32[2048]{0:T(1024)} %param.22) | copy-start | bytes 24580
Sparse Core Ops, SparseCore 0:
  30.9 34.4 all-gather.2
where the time goes:
time: 310 us; the launch traced here: 309 us
  Pallas kernels  194 us (63%)
  waiting for transfers between devices  42.2 us (14%)
  local copies, waits for them, and re-layouts  22.7 us (7%)
  blocking collectives  17.1 us (6%)
  between operations  13.7 us (4%)
  starting transfers between devices  8.24 us (3%)
  other arithmetic  8.21 us (3%)
    pallas_call x1, Pallas kernels, at_experts(): pl.pallas_call(experts_kernel, out_shape=jax.ShapeDtypeStruct(outbound.sh...  164 us
    all_gather x1, waiting for transfers between devices, on_device(): lax.all_gather(arrived[:, :BLK + EXTRA], 'sp', axis=0, axis_index_groups=...  29.8 us
    pallas_call x1, Pallas kernels, attend(): pl.pallas_call(attention_kernel, out_shape=jax.ShapeDtypeStruct((groups,...  29.8 us
    all_to_all x1, blocking collectives, on_device(): lax.all_to_all(payload, 'sp', split_axis=0, concat_axis=0, axis_index_gro...  17.1 us
    all_to_all x1, waiting for transfers between devices, on_device(): lax.all_to_all(normed, 'tp', split_axis=1, concat_axis=0, tiled=True)  6.91 us
  transfers between devices with their start and end apart: 3, of which 3 were waited for; matrix products, arithmetic and copies ran while one was open for 2% of the time, Pallas kernels for 0%

commit v1 on v0

--- a/solution.py
+++ b/solution.py
@@ -114,7 +114,9 @@
         out = acc[16:80, :] / acc[0:1, :]
         mean_square = jnp.mean(out * out, axis=0, keepdims=True)
         gain = jnp.concatenate([gain_ref[...]] * 4, axis=1)
-        o_ref[i] = (out * lax.rsqrt(mean_square + EPS) * gain).astype(BF16)
+        normed = (out * lax.rsqrt(mean_square + EPS) * gain).astype(BF16)
+        for c in range(4):
+            o_ref[i, c] = normed[:, c * 128 : (c + 1) * 128]
         return unused
 
     lax.fori_loop(0, groups, one_query_block, 0)
@@ -126,7 +128,7 @@
     vmem = pl.BlockSpec(memory_space=pltpu.VMEM)
     return pl.pallas_call(
         attention_kernel,
-        out_shape=jax.ShapeDtypeStruct((groups, 64, BLK), BF16),
+        out_shape=jax.ShapeDtypeStruct((groups, 4, 64, 128), BF16),
         in_specs=[vmem] * 3,
         out_specs=vmem,
         scratch_shapes=[
@@ -144,28 +146,189 @@
 
 MESH = pl.DeviceIdType.MESH
 GROUP = 4
+KVX = BLK + EXTRA
+
+
+def remote(src, dst, send_sem, recv_sem, sp, tp):
+    return pltpu.make_async_remote_copy(
+        src_ref=src,
+        dst_ref=dst,
+        send_sem=send_sem,
+        recv_sem=recv_sem,
+        device_id=(sp, tp),
+        device_id_type=MESH,
+    )
+
+
+def gather_kernel(
+    pay_ref, q_ref, kvx_ref, q_send, q_recv, a_send, a_recv, y_send, y_recv,
+    h_send, h_recv, d_send, d_recv,
+):
+    members, groups = kvx_ref.shape[:2]
+    ring = members // 2
+    s = lax.axis_index("sp")
+    t = lax.axis_index("tp")
+    z, j = s // members, lax.rem(s, members)
+    y, core = j // 2, lax.rem(j, 2)
+
+    def member(dy, other=0):
+        c = 1 - core if other else core
+        return lax.rem(y + dy + ring, ring) * 2 + c
+
+    sides = (member(1), member(-1))
+    far = member(2)
+    peers = [lax.rem(z + d, groups) * members + j for d in range(1, groups)]
+    peers += [z * members + m for m in (*sides, member(0, 1))]
+    barrier = pltpu.get_barrier_semaphore()
+    for peer in peers:
+        pl.semaphore_signal(barrier, 1, device_id=(peer, t), device_id_type=MESH)
+    pl.semaphore_wait(barrier, len(peers))
+
+    order = (0, 1, 3, 2)
+
+    def kv_copy(n, d, source):
+        to = lax.rem(z + d, groups)
+        return remote(
+            pay_ref.at[to, pl.ds(0, KVX)], kvx_ref.at[j, source], a_send, a_recv.at[n],
+            to * members + j, t,
+        )
+
+    def q_copy(n, d, source):
+        to = lax.rem(z + d, groups)
+        return remote(
+            pay_ref.at[to, pl.ds(KVX, BLK // 2)], q_ref.at[source], q_send, q_recv.at[n],
+            to * members + j, t,
+        )
+
+    for n, d in enumerate(order):
+        if d:
+            kv_copy(n, d, z).start()
+    for n, d in enumerate(order):
+        if d:
+            q_copy(n, d, z).start()
+    kvx_ref[j, z] = pay_ref[z, 0:KVX, :]
+    q_ref[z] = pay_ref[z, KVX : KVX + BLK // 2, :]
+
+    def source_of(n):
+        return lax.rem(z - order[n] + groups, groups)
+
+    def to_side(i, rows, send_sem, recv_sem):
+        return remote(rows, rows, send_sem, recv_sem, z * members + sides[i], t)
+
+    def to_core(kind, n, m):
+        rows = kvx_ref.at[m, source_of(n)]
+        return remote(
+            rows, rows, d_send, d_recv.at[kind, n], z * members + member(0, 1), t
+        )
+
+    def piece(i):
+        return pl.ds(i * (KVX // 2), KVX // 2)
+
+    def enter(n):
+        if n:
+            kv_copy(n, order[n], source_of(n)).wait_recv()
+        rows = kvx_ref.at[j, source_of(n)]
+        for i in range(2):
+            to_side(i, rows, y_send.at[i], y_recv.at[i, n]).start()
+        to_core(0, n, j).start()
+
+    def relay(n):
+        for i in range(2):
+            origin = sides[1 - i]
+            rows = kvx_ref.at[origin, source_of(n)]
+            to_side(i, rows, y_send.at[i], y_recv.at[i, n]).wait_recv()
+            rows = kvx_ref.at[origin, source_of(n), piece(i)]
+            to_side(i, rows, h_send.at[i], h_recv.at[i, n]).start()
+            to_core(1 + i, n, origin).start()
+
+    def finish(n):
+        for i in range(2):
+            rows = kvx_ref.at[far, source_of(n), piece(i)]
+            to_side(i, rows, h_send.at[i], h_recv.at[i, n]).wait_recv()
+        to_core(3, n, far).start()
+
+    for step in range(groups + 2):
+        if step < groups:
+            enter(step)
+        if 1 <= step <= groups:
+            relay(step - 1)
+        if step >= 2:
+            finish(step - 2)
+    for n in range(groups):
+        for kind in range(4):
+            to_core(kind, n, member((0, -1, 1, 2)[kind], 1)).wait_recv()
+    for n in range(1, groups):
+        q_copy(n, order[n], source_of(n)).wait_recv()
+    for n in range(1, groups):
+        kv_copy(n, order[n], z).wait_send()
+        q_copy(n, order[n], z).wait_send()
+    rows = kvx_ref.at[j]
+    halves = kvx_ref.at[0, :, pl.ds(0, KVX // 2)]
+    for i in range(2):
+        to_side(i, rows, y_send.at[i], y_recv.at[i, 0]).wait_send()
+        to_side(i, halves, h_send.at[i], h_recv.at[i, 0]).wait_send()
+    every = kvx_ref.at[pl.ds(0, 4)]
+    remote(every, every, d_send, d_recv.at[0, 0], z * members, t).wait_send()
+
+
+def gather_history(payload, members):
+    groups = payload.shape[0]
+    vmem = pl.BlockSpec(memory_space=pltpu.VMEM)
+    dma = pltpu.SemaphoreType.DMA
+    return pl.pallas_call(
+        gather_kernel,
+        out_shape=(
+            jax.ShapeDtypeStruct((groups, BLK // 2, 128), BF16),
+            jax.ShapeDtypeStruct((members, groups, KVX, 128), BF16),
+        ),
+        in_specs=[vmem],
+        out_specs=(vmem, vmem),
+        scratch_shapes=[
+            dma,
+            dma((groups,)),
+            dma,
+            dma((groups,)),
+            dma((2,)),
+            dma((2, groups)),
+            dma((2,)),
+            dma((2, groups)),
+            dma,
+            dma((4, groups)),
+        ],
+        compiler_params=pltpu.CompilerParams(
+            collective_id=0, has_side_effects=True, vmem_limit_bytes=16 * 1024 * 1024
+        ),
+        name="gather_history",
+    )(payload)
 
 
 def experts_kernel(
-    out_ref, wg_hbm, wu_hbm, wd_hbm, ret_ref,
-    x, p, r_in, m_in, wg, wu, wd,
-    w_sem, a2a_send, a2a_recv, ag_send, ag_recv, relay_send, relay_recv,
+    normed_ref, ow_hbm, resid_ref, ng_ref, rows_ref, cols_ref, rw_ref, wg_hbm, wu_hbm, wd_hbm,
+    mixed_ref,
+    heads, ow, stream, out_ref, ret_ref, x, p, r_in, m_in, wg, wu, wd,
+    w_sem, head_send, head_recv, a2a_send, a2a_recv, ag_send, ag_recv, relay_send, relay_recv,
     r_send, r_recv, m_send, m_recv, ret_send, ret_recv,
 ):
     experts, slots, width = out_ref.shape
+    groups = normed_ref.shape[0]
     tps = x.shape[0]
+    members = experts // groups
     steps = experts // GROUP
     half = GROUP // 2
+    send = remote
     s = lax.axis_index("sp")
     t = lax.axis_index("tp")
+    z, j = s // members, lax.rem(s, members)
     right = lax.rem(t + 1, tps)
     left = lax.rem(t + tps - 1, tps)
     far = lax.rem(t + 2, tps)
     sides = (right, left)
 
     loads = [
-        pltpu.make_async_copy(a.at[0], b, w_sem.at[i])
-        for i, (a, b) in enumerate(((wg_hbm, wg), (wu_hbm, wu), (wd_hbm, wd)))
+        pltpu.make_async_copy(a, b, w_sem.at[i])
+        for i, (a, b) in enumerate(
+            ((ow_hbm, ow), (wg_hbm.at[0], wg), (wu_hbm.at[0], wu), (wd_hbm.at[0], wd))
+        )
     ]
     for load in loads:
         load.start()
@@ -180,17 +343,46 @@
 
     for side in sides:
         pl.semaphore_signal(barrier, 1, device_id=(s, side), device_id_type=MESH)
-    pl.semaphore_wait(barrier, experts - 1 + 2)
-
-    def send(src, dst, send_sem, recv_sem, sp, tp):
-        return pltpu.make_async_remote_copy(
-            src_ref=src,
-            dst_ref=dst,
-            send_sem=send_sem,
-            recv_sem=recv_sem,
-            device_id=(sp, tp),
-            device_id_type=MESH,
-        )
+
+    def owner(n):
+        return lax.rem(z + n // tps, groups), lax.rem(t + lax.rem(n, tps), tps)
+
+    @pl.loop(1, groups * tps)
+    def _(n):
+        zz, tt = owner(n)
+        pl.semaphore_signal(barrier, 1, device_id=(zz * members + j, tt), device_id_type=MESH)
+
+    pl.semaphore_wait(barrier, experts - 1 + 2 + groups * tps - 1)
+
+    mine = t * groups + z
+
+    @pl.loop(1, groups * tps)
+    def _(n):
+        zz, tt = owner(n)
+        send(
+            normed_ref.at[zz, tt], heads.at[mine], head_send, head_recv, zz * members + j, tt
+        ).start()
+
+    heads[mine] = normed_ref[z, t]
+    slot_ids = lax.broadcasted_iota(jnp.int32, (experts * slots, 128), 0)
+    chosen = (slot_ids == rows_ref[0:1, :]) | (slot_ids == rows_ref[1:2, :])
+    chosen = jnp.where(chosen, 1.0, 0.0).astype(BF16)
+    loads[0].wait()
+    others = heads.at[pl.ds(0, groups * tps - 1)]
+    send(others, others, head_send, head_recv, s, right).wait()
+    projected = lax.dot_general(
+        heads[...].reshape(groups * tps * 64, 128), ow[...], (((0,), (0,)), ((), ())),
+        preferred_element_type=F32,
+    )
+    stream[...] = (resid_ref[...].astype(F32) + projected).astype(BF16)
+    widened = stream[...].astype(F32)
+    mean_wide = jnp.mean(widened * widened, axis=-1, keepdims=True)
+    expert_input = (widened * lax.rsqrt(mean_wide + EPS) * ng_ref[...]).astype(BF16)
+    out_ref[...] = (
+        jnp.dot(chosen, expert_input, preferred_element_type=F32)
+        .astype(BF16)
+        .reshape(experts, slots, width)
+    )
 
     def to_side(i, src, dst, send_sem, recv_sem):
         return send(src, dst, send_sem, recv_sem, s, sides[i])
@@ -296,7 +488,7 @@
 
         @pl.when(i == 2)
         def _():
-            for load in loads:
+            for load in loads[1:]:
                 load.wait()
 
         @pl.when((i >= 2) & (i < steps + 2))
@@ -314,22 +506,40 @@
         to_side(i, some, some, relay_send.at[i], relay_recv.at[i, 0]).wait_send()
         to_side(i, some, some, r_send.at[i], r_recv.at[i, 0]).wait_send()
         to_side(i, every, every, m_send.at[i], m_recv.at[i, 0]).wait_send()
-
-
-def at_experts(outbound, w_gate, w_up, w_down):
-    experts, slots, width = outbound.shape
+    lanes = lax.broadcasted_iota(jnp.int32, (128, experts * slots), 1)
+    spread = jnp.where(lanes == cols_ref[:, 0:1], rw_ref[:, 0:1], 0.0) + jnp.where(
+        lanes == cols_ref[:, 1:2], rw_ref[:, 1:2], 0.0
+    )
+    results = ret_ref[...].reshape(experts * slots, width)
+    mixed = stream[...].astype(F32)
+    for _ in range(3):
+        digit = spread.astype(BF16)
+        mixed = mixed + jnp.dot(digit, results, preferred_element_type=F32)
+        spread = spread - digit.astype(F32)
+    mixed_ref[...] = mixed.astype(BF16)
+
+
+def at_experts(normed, out_weight, resid, norm_gain, targets, route_weights, w_gate, w_up, w_down):
+    groups, tps = normed.shape[:2]
+    rows, width = resid.shape
     hidden = w_gate.shape[2]
-    tps = lax.axis_size("tp")
+    experts = lax.axis_size("sp")
+    slots = 16
     steps = experts // GROUP
     vmem = pl.BlockSpec(memory_space=pltpu.VMEM)
     hbm = pl.BlockSpec(memory_space=pl.ANY)
     dma = pltpu.SemaphoreType.DMA
     return pl.pallas_call(
         experts_kernel,
-        out_shape=jax.ShapeDtypeStruct(outbound.shape, BF16),
-        in_specs=[vmem, hbm, hbm, hbm],
+        out_shape=jax.ShapeDtypeStruct((rows, width), BF16),
+        in_specs=[vmem, hbm, vmem, vmem, vmem, vmem, vmem, hbm, hbm, hbm],
         out_specs=vmem,
         scratch_shapes=[
+            pltpu.VMEM((groups * tps, 64, 128), BF16),
+            pltpu.VMEM(out_weight.shape, BF16),
+            pltpu.VMEM((rows, width), BF16),
+            pltpu.VMEM((experts, slots, width), BF16),
+            pltpu.VMEM((experts, slots, width), BF16),
             pltpu.VMEM((tps, experts, slots, width), BF16),
             pltpu.VMEM((tps, experts, slots, width), BF16),
             pltpu.VMEM((2, experts // 2, slots, width), BF16),
@@ -337,7 +547,9 @@
             pltpu.VMEM((width, hidden), BF16),
             pltpu.VMEM((width, hidden), BF16),
             pltpu.VMEM((hidden, width), BF16),
-            dma((3,)),
+            dma((4,)),
+            dma,
+            dma,
             dma,
             dma((steps,)),
             dma((2,)),
@@ -352,10 +564,13 @@
             dma,
         ],
         compiler_params=pltpu.CompilerParams(
-            collective_id=1, has_side_effects=True, vmem_limit_bytes=58 * 1024 * 1024
+            collective_id=1, has_side_effects=True, vmem_limit_bytes=60 * 1024 * 1024
         ),
         name="experts",
-    )(outbound, w_gate, w_up, w_down)
+    )(
+        normed, out_weight, resid, norm_gain.reshape(1, width), targets.T, targets, route_weights,
+        w_gate, w_up, w_down,
+    )
 
 
 def on_device(
@@ -393,49 +608,18 @@
     zero_row = jnp.pad(jnp.stack(pieces_of(gate0), axis=2), ((0, 0), (0, 15), (0, 125)))
     extra = jnp.concatenate([rel, docs, zero_row], axis=1).astype(BF16)
     payload = jnp.concatenate([kv, extra, q_pack], axis=1)
-    columns = [[j + members * g for g in range(heads)] for j in range(members)]
-    rows = [[j + members * g for j in range(members)] for g in range(heads)]
-    arrived = lax.all_to_all(
-        payload, "sp", split_axis=0, concat_axis=0, axis_index_groups=columns, tiled=True
-    )
-    kvx = lax.all_gather(arrived[:, : BLK + EXTRA], "sp", axis=0, axis_index_groups=rows)
+    q, kvx = gather_history(payload, members)
     gain = jnp.broadcast_to(lax.dynamic_slice_in_dim(head_gain, z * 64, 64)[:, None], (64, 128))
-    normed = attend(arrived[:, BLK + EXTRA :], kvx, gain)
-    normed = lax.all_to_all(
-        normed, "sp", split_axis=0, concat_axis=0, axis_index_groups=columns, tiled=True
-    ).reshape(heads * 64, tokens)
-    tp_count = lax.axis_size("tp")
-    local_rows = tokens // tp_count
-    regrouped = lax.all_to_all(normed, "tp", split_axis=1, concat_axis=0, tiled=True)
-    projected = lax.dot_general(
-        regrouped, out_weight, (((0,), (0,)), ((), ())), preferred_element_type=F32
-    )
-    stream = lax.optimization_barrier((resid.astype(F32) + projected).astype(BF16))
-    widened = stream.astype(F32)
-    mean_wide = jnp.mean(widened * widened, axis=-1, keepdims=True)
-    expert_input = (widened * lax.rsqrt(mean_wide + EPS) * norm_gain).astype(BF16)
-    top_count = routes.shape[1]
-    expert_count = sp_count
-    model_width = stream.shape[1]
-    capacity = 2 * top_count * tokens // (tp_count * expert_count)
+    normed = attend(q, kvx, gain)
     flat_routes = routes.reshape(-1)
-    route_total = flat_routes.shape[0]
-    onehot = (flat_routes[:, None] == jnp.arange(expert_count, dtype=jnp.int32)[None, :]).astype(
+    onehot = (flat_routes[:, None] == jnp.arange(sp_count, dtype=jnp.int32)[None, :]).astype(
         jnp.int32
     )
     ranks = jnp.sum(jnp.cumsum(onehot, axis=0) * onehot, axis=1) - 1
-    targets = flat_routes * capacity + ranks
-    owners = jnp.arange(route_total, dtype=jnp.int32) // top_count
-    slot_owner = jnp.zeros((expert_count * capacity,), jnp.int32).at[targets].set(owners)
-    slot_used = jnp.zeros((expert_count * capacity,), jnp.bool_).at[targets].set(True)
-    outbound = jnp.where(slot_used[:, None], expert_input[slot_owner], jnp.zeros((), BF16))
-    outbound = outbound.reshape(expert_count, capacity, model_width)
-
-    returned = at_experts(outbound, w_gate, w_up, w_down)
-    results = returned.reshape(expert_count * capacity, model_width)[targets]
-    results = results.reshape(local_rows, top_count, model_width)
-    mixed = widened + jnp.sum(route_weights[:, :, None] * results.astype(F32), axis=1)
-    return mixed.astype(BF16)
+    targets = (flat_routes * 16 + ranks).reshape(routes.shape)
+    return at_experts(
+        normed, out_weight, resid, norm_gain, targets, route_weights, w_gate, w_up, w_down
+    )
 
 
 def solution(mesh):

time: 310 us -> 252 us (0.81)
  waiting for transfers between devices: 42.2 us -> 0 us
  Pallas kernels: 194 us -> 236 us
  blocking collectives: 17.1 us -> 0 us
  between operations: 13.7 us -> 0.25 us
  local copies, waits for them, and re-layouts: 22.7 us -> 13.2 us
  starting transfers between devices: 8.24 us -> 0 us
  other arithmetic: 8.21 us -> 1.53 us
    pallas_call x1 -> x2, Pallas kernels: 164 us -> 209 us  [the longest x1 177 us: at_experts(): pl.pallas_call(experts_kernel, out_shape=jax.ShapeDtypeStruct((rows, widt...]
    all_gather x1 -> x0, waiting for transfers between devices: 29.8 us -> none  [on_device(): lax.all_gather(arrived[:, :BLK + EXTRA], 'sp', axis=0, axis_index_groups=...]
    all_to_all x1 -> x0, blocking collectives: 17.1 us -> none  [on_device(): lax.all_to_all(payload, 'sp', split_axis=0, concat_axis=0, axis_index_gro...]
    all_to_all x2 -> x0, waiting for transfers between devices: 12.4 us -> none  [the longest x1 6.91 us: on_device(): lax.all_to_all(normed, 'tp', split_axis=1, concat_axis=0, tiled=True)]
    all_to_all x2 -> x0, starting transfers between devices: 8.23 us -> none  [the longest x1 4.27 us: on_device(): lax.all_to_all(normed, 'sp', split_axis=0, concat_axis=0, axis_index_grou...]
    gather x2 -> x0, local copies, waits for them, and re-layouts: 7.67 us -> none  [the longest x1 5.21 us: on_device(): results = returned.reshape(expert_count * capacity, model_width)[targets]]
    unnamed x23 -> x26, local copies, waits for them, and re-layouts: 4.87 us -> 10.1 us
    reduce_sum x2 -> x0, other arithmetic: 3.35 us -> none  [the longest x1 3.16 us: on_device(): jnp.sum(route_weights[:, :, None] * results.astype(F32), axis=1)]
  transfers between devices with their start and end apart: 3 -> 0, of which waited for: 3 -> 0; matrix products, arithmetic and copies ran while one was open for 2% -> 0% of each run, Pallas kernels for 0% -> 0%
where the time goes in v1:
time: 252 us; the launch traced here: 251 us
  Pallas kernels  236 us (94%)
  local copies, waits for them, and re-layouts  13.2 us (5%)
    pallas_call x1, Pallas kernels, at_experts(): pl.pallas_call(experts_kernel, out_shape=jax.ShapeDtypeStruct((rows, widt...  177 us
    pallas_call x1, Pallas kernels, gather_history(): pl.pallas_call(gather_kernel, out_shape=(jax.ShapeDtypeStruct((groups, BL...  31.6 us
    pallas_call x1, Pallas kernels, attend(): pl.pallas_call(attention_kernel, out_shape=jax.ShapeDtypeStruct((groups,...  27.8 us
    unnamed x26, local copies, waits for them, and re-layouts  10.1 us

profile of v1, /device:TPU:1, one launch (start us, length us, event | category | flops | bytes accessed | tf_op | source)
XLA Modules:
  0.0 251.2 jit_solution(13461008061715120897)
XLA Ops:
  0.0 1.1 copy.42
  1.1 0.3 copy.43
  1.4 1.1 copy.40
  2.5 0.3 copy.41
  2.8 0.3 pad_maximum_fusion
  3.1 0.1 slice_reduce_fusion.1
  3.2 0.1 fusion.13
  3.4 0.1 fusion.18
  3.8 0.1 fusion.11
  3.9 0.1 copy.48
  4.0 0.3 copy.49
  4.4 0.1 pad_maximum_fusion.1
  4.5 0.3 concatenate.14.pay_ref
  4.9 31.6 %gather_history.1 = (bf16[4,256,128]{2,1,0:T(8,128)(2,1)S(1)}, bf16[8,4,544,128]{3,2,1,0:T(8,128)(2,1)S(1)}) custom-call(bf16[4,800,128]{2,1,0:T(8,128)(2,1)S(1)} %concatenate.14.pay_ref), custom_call_target="tpu_custom_call" | custom-call | tf_op jit(solution)/shard_map/gather_history/pallas_call | solution.py:278
  36.5 2.0 copy-done
  38.5 0.1 dynamic_slice.3
  38.6 0.1 broadcast_in_dim.16.gain_ref
  38.7 2.3 copy-done.1
  41.0 27.8 %attention.1.normed_ref = bf16[4,4,64,128]{3,2,1,0:T(8,128)(2,1)S(1)} custom-call(bf16[4,256,128]{2,1,0:T(8,128)(2,1)S(1)} %get-tuple-element.7.q_ref, bf16[8,4,544,128]{3,2,1,0:T(8,128)(2,1)S(1)} %copy-done.1, f32[64,128]{1,0:T(8,128)S(1)} %broadcast_in_dim.16.gain_ref), custom_call_target="tpu_custom_call" | custom-call | tf_op jit(solution)/shard_map/attention/pallas_call | solution.py:129
  68.7 0.7 copy-done.2
  69.4 0.1 copy.53
  69.5 0.1 copy.50
  69.7 0.1 eq.25
  69.8 0.1 eq.29
  70.0 0.6 reduce-window.6
  70.5 0.2 slice_reduce_fusion
  70.8 0.1 fusion.1
  70.9 0.1 sub.41
  71.1 0.6 copy.54.rows_ref
  71.7 0.7 copy.55.rw_ref
  72.4 176.9 %experts.1 = bf16[128,2048]{1,0:T(8,128)(2,1)} custom-call(bf16[4,4,64,128]{3,2,1,0:T(8,128)(2,1)} %copy-done.2, bf16[1024,2048]{1,0:T(8,128)(2,1)} %ow_hbm.1, bf16[128,2048]{1,0:T(8,128)(2,1)} %resid_ref.1, f32[1,2048]{1,0:T(1,128)} %bitcast.44, s32[2,128]{1,0:T(2,128)} %copy.54.rows_ref, s32[128,2]{1,0:T(8,128)} %copy-done.3, f32[128,2]{1,0:T(8,128)} %copy.55.rw_ref, ...), custom_call_target="tpu_custom_call" | custom-call | tf_op jit(solution)/shard_map/experts/pallas_call | solution.py:532
  249.3 1.9 copy.59
  (32 shorter events, 0.4 us)
Async XLA Ops:
  0.0 3.1 %copy-start.5 = (f32[512,4]{0,1:T(4,128)S(1)}, f32[512,4]{0,1:T(4,128)}, u32[]{:S(2)}) copy-start(f32[512,4]{0,1:T(4,128)} %param.17) | copy-start | bytes 24580
  0.0 3.4 %copy-start.7 = (s32[512]{0:T(512)S(1)}, s32[512]{0:T(512)}, u32[]{:S(2)}) copy-start(s32[512]{0:T(512)} %param.18) | copy-start | bytes 6148
  0.0 3.9 %copy-start.4 = (bf16[512,256]{1,0:T(8,128)(2,1)S(1)}, bf16[512,256]{1,0:T(8,128)(2,1)}, u32[]{:S(2)}) copy-start(bf16[512,256]{1,0:T(8,128)(2,1)} %param.14) | copy-start | bytes 786436
  2.8 35.7 %copy-start.9 = (f32[256]{0:T(256)S(1)}, f32[256]{0:T(256)}, u32[]{:S(2)}) copy-start(f32[256]{0:T(256)} %param.19) | copy-start | bytes 3076
  4.5 64.9 %copy-start.6 = (s32[128,2]{0,1:T(2,128)S(1)}, s32[128,2]{0,1:T(2,128)}, u32[]{:S(2)}) copy-start(s32[128,2]{0,1:T(2,128)} %param.23) | copy-start | bytes 3076
  4.9 66.8 %copy-start.8 = (f32[128,2]{0,1:T(2,128)S(1)}, f32[128,2]{0,1:T(2,128)}, u32[]{:S(2)}) copy-start(f32[128,2]{0,1:T(2,128)} %param.24) | copy-start | bytes 3076
  36.5 2.0 copy-start
  38.7 2.3 copy-start.1
  68.7 0.7 copy-start.2
  71.1 1.4 copy-start.3

commit v2 on v1

--- a/solution.py
+++ b/solution.py
@@ -15,24 +15,78 @@
 
 
 def pieces_of(x):
-    hi = lax.reduce_precision(x, 8, 7)
+    hi = x.astype(BF16).astype(F32)
     rest = x - hi
-    mid = lax.reduce_precision(rest, 8, 7)
+    mid = rest.astype(BF16).astype(F32)
     return hi, mid, rest - mid
 
 
-def attention_kernel(q_ref, kvx_ref, gain_ref, o_ref, kp, vt, qp, acc, mrow, g0):
+def pack(queries_ref, keys_ref, values_ref, gate_ref, doc_ref, pay_ref):
+    lane = lax.broadcasted_iota(jnp.int32, (BLK, 128), 1)
+    half = lane[: BLK // 2]
+    row_lane = lane[:1]
+    docs = doc_ref[...].astype(F32)
+    for h in range(pay_ref.shape[0]):
+        at = slice(h // 2 * 128, h // 2 * 128 + 128)
+        k = keys_ref[:, at].astype(F32)
+        v = values_ref[:, at].astype(F32)
+        q = queries_ref[:, at].astype(F32)
+        q0, q1 = q[: BLK // 2], q[BLK // 2 :]
+        if h % 2:
+            k, q0 = pltpu.roll(k, 64, 1), pltpu.roll(q0, 64, 1)
+        else:
+            v, q1 = pltpu.roll(v, 64, 1), pltpu.roll(q1, 64, 1)
+        pay_ref[h, 0:BLK, :] = jnp.where(lane < 64, k, v).astype(BF16)
+        pay_ref[h, BLK + EXTRA :, :] = jnp.where(half < 64, q0, q1).astype(BF16)
+        gate = gate_ref[h : h + 1, :]
+        base = gate[:, 0:1]
+        rows = [
+            p[:, c * 128 : (c + 1) * 128]
+            for p in pieces_of((base - gate) * LOG2E)
+            for c in range(4)
+        ]
+        rows += [docs[:, c * 128 : (c + 1) * 128] for c in range(4)]
+        b0, b1, b2 = pieces_of(jnp.broadcast_to(base, (1, 128)))
+        rows.append(
+            jnp.where(
+                row_lane == 0,
+                b0,
+                jnp.where(row_lane == 1, b1, jnp.where(row_lane == 2, b2, 0.0)),
+            )
+        )
+        rows.append(jnp.zeros((15, 128), F32))
+        pay_ref[h, BLK : BLK + EXTRA, :] = jnp.concatenate(rows, axis=0).astype(BF16)
+
+
+def attention_kernel(
+    q_hbm, kvx_hbm, gain_ref, o_ref, q_ref, kvx_ref, kp, vt, qp, score_ref, acc, mrow, g0, q_sem, kv_sem
+):
     members = kvx_ref.shape[0]
     groups = kvx_ref.shape[1]
     blocks = members * groups
     me = lax.rem(lax.axis_index("sp"), members)
+    z = lax.axis_index("sp") // members
     lane = lax.broadcasted_iota(jnp.int32, (128, 128), 1)
     lane_wide = lax.broadcasted_iota(jnp.int32, (BLK, 128), 1)
     row_extra = lax.broadcasted_iota(jnp.int32, (EXTRA, 128), 0)
     is_doc = (row_extra >= 12) & (row_extra < 16)
 
+    def fetch(kb):
+        member, group = lax.rem(kb, members), kb // members
+        return pltpu.make_async_copy(
+            kvx_hbm.at[member, group], kvx_ref.at[member, group], kv_sem.at[kb]
+        )
+
+    @pl.loop(0, blocks)
+    def _(kb):
+        fetch(kb).start()
+
+    q_copy = pltpu.make_async_copy(q_hbm, q_ref, q_sem)
+    q_copy.start()
+
     def prepare(kb, counts):
         member, group = lax.rem(kb, members), kb // members
+        fetch(kb).wait()
         extra = kvx_ref[member, group, BLK : BLK + EXTRA, :].astype(F32)
         g0[kb] = jnp.sum(jnp.where(row_extra == 16, extra, 0.0))
         counts = tuple(
@@ -52,6 +106,9 @@
 
     zero = jnp.zeros((EXTRA, 128), F32)
     counts = lax.fori_loop(0, blocks, prepare, (zero, zero, zero))
+    q_copy.wait()
+    gains = jnp.broadcast_to(gain_ref[pl.ds(z // 2, 1), :], (128, 128)).T
+    gain_column = jnp.where(lax.rem(z, 2) == 0, gains[0:64], gains[64:128])
     starts = [jnp.sum(c).astype(jnp.int32) for c in counts]
 
     def one_query_block(i, unused):
@@ -73,47 +130,57 @@
         last = jnp.max(start)
         base = g0[qb]
 
-        def visit(kb, masked, fresh):
-            shift = (base - g0[kb]) * LOG2E
-            scores = lax.dot_general(
+        first_block = first // BLK
+        count = qb - first_block + 1
+
+        def block_at(n):
+            return jnp.where(n == 0, qb, jnp.minimum(first_block + n - 1, qb))
+
+        def score_of(kb):
+            return lax.dot_general(
                 kp[kb], qp[...], (((1,), (1,)), ((), ())), preferred_element_type=F32
             )
+
+        def visit(slot, n, masked):
+            kb = block_at(n)
+            shift = (base - g0[kb]) * LOG2E
+            scores = score_ref[slot]
             if masked:
                 key_pos = kb * BLK + lax.broadcasted_iota(jnp.int32, (BLK, BLK), 0)
                 query_pos = qb * BLK + lax.broadcasted_iota(jnp.int32, (BLK, BLK), 1)
                 allowed = (key_pos <= query_pos) & (key_pos >= start)
                 scores = jnp.where(allowed, scores, NEG)
-            top = jnp.max(scores, axis=0, keepdims=True) + shift
-            if not fresh:
-                old = mrow[...]
-                top = jnp.maximum(old, top)
+            old = mrow[...]
+            top = jnp.maximum(old, jnp.max(scores, axis=0, keepdims=True) + shift)
+            score_ref[1 - slot] = score_of(block_at(n + 1))
             weights = jnp.exp2(scores - (top - shift)).astype(BF16)
             added = jnp.dot(vt[kb], weights, preferred_element_type=F32)
-            if fresh:
-                acc[...] = added
-            else:
-                acc[...] = acc[...] * jnp.exp2(old - top) + added
+            acc[...] = acc[...] * jnp.exp2(old - top) + added
             mrow[...] = top
 
-        visit(qb, True, True)
-
-        def earlier(kb, carry):
-            plain = kb * BLK >= last
-
-            @pl.when(plain)
-            def _():
-                visit(kb, False, False)
-
-            @pl.when(jnp.logical_not(plain))
-            def _():
-                visit(kb, True, False)
+        mrow[...] = jnp.full((1, BLK), NEG, F32)
+        acc[...] = jnp.zeros((80, BLK), F32)
+        score_ref[0] = score_of(qb)
+
+        def two_blocks(m, carry):
+            for slot in range(2):
+                n = 2 * m + slot
+                plain = (n > 0) & (block_at(n) * BLK >= last)
+
+                @pl.when((n < count) & plain)
+                def _():
+                    visit(slot, n, False)
+
+                @pl.when((n < count) & jnp.logical_not(plain))
+                def _():
+                    visit(slot, n, True)
 
             return carry
 
-        lax.fori_loop(first // BLK, qb, earlier, 0)
+        lax.fori_loop(0, (count + 1) // 2, two_blocks, 0)
         out = acc[16:80, :] / acc[0:1, :]
         mean_square = jnp.mean(out * out, axis=0, keepdims=True)
-        gain = jnp.concatenate([gain_ref[...]] * 4, axis=1)
+        gain = jnp.concatenate([gain_column] * 4, axis=1)
         normed = (out * lax.rsqrt(mean_square + EPS) * gain).astype(BF16)
         for c in range(4):
             o_ref[i, c] = normed[:, c * 128 : (c + 1) * 128]
@@ -126,18 +193,24 @@
     members, groups = kvx.shape[:2]
     blocks = members * groups
     vmem = pl.BlockSpec(memory_space=pltpu.VMEM)
+    hbm = pl.BlockSpec(memory_space=pl.ANY)
     return pl.pallas_call(
         attention_kernel,
         out_shape=jax.ShapeDtypeStruct((groups, 4, 64, 128), BF16),
-        in_specs=[vmem] * 3,
+        in_specs=[hbm, hbm, vmem],
         out_specs=vmem,
         scratch_shapes=[
+            pltpu.VMEM(q.shape, BF16),
+            pltpu.VMEM(kvx.shape, BF16),
             pltpu.VMEM((blocks, BLK, 256), BF16),
             pltpu.VMEM((blocks, 80, BLK), BF16),
             pltpu.VMEM((BLK, 256), BF16),
+            pltpu.VMEM((2, BLK, BLK), F32),
             pltpu.VMEM((80, BLK), F32),
             pltpu.VMEM((1, BLK), F32),
             pltpu.SMEM((blocks,), F32),
+            pltpu.SemaphoreType.DMA,
+            pltpu.SemaphoreType.DMA((blocks,)),
         ],
         compiler_params=pltpu.CompilerParams(vmem_limit_bytes=48 * 1024 * 1024),
         name="attention",
@@ -145,7 +218,7 @@
 
 
 MESH = pl.DeviceIdType.MESH
-GROUP = 4
+GROUP = 2
 KVX = BLK + EXTRA
 
 
@@ -161,11 +234,26 @@
 
 
 def gather_kernel(
-    pay_ref, q_ref, kvx_ref, q_send, q_recv, a_send, a_recv, y_send, y_recv,
+    queries_hbm, keys_hbm, values_hbm, gate_hbm, doc_hbm, q_ref, kvx_ref,
+    queries_ref, keys_ref, values_ref, gate_ref, doc_ref, in_sem, pay_ref, q_send, q_recv, a_send, a_recv, y_send, y_recv,
     h_send, h_recv, d_send, d_recv,
 ):
     members, groups = kvx_ref.shape[:2]
     ring = members // 2
+    loads = [
+        pltpu.make_async_copy(a, b, in_sem.at[i])
+        for i, (a, b) in enumerate(
+            (
+                (queries_hbm, queries_ref),
+                (keys_hbm, keys_ref),
+                (values_hbm, values_ref),
+                (gate_hbm, gate_ref),
+                (doc_hbm, doc_ref),
+            )
+        )
+    ]
+    for load in loads:
+        load.start()
     s = lax.axis_index("sp")
     t = lax.axis_index("tp")
     z, j = s // members, lax.rem(s, members)
@@ -182,6 +270,9 @@
     barrier = pltpu.get_barrier_semaphore()
     for peer in peers:
         pl.semaphore_signal(barrier, 1, device_id=(peer, t), device_id_type=MESH)
+    for load in loads:
+        load.wait()
+    pack(queries_ref, keys_ref, values_ref, gate_ref, doc_ref, pay_ref)
     pl.semaphore_wait(barrier, len(peers))
 
     order = (0, 1, 3, 2)
@@ -271,8 +362,8 @@
     remote(every, every, d_send, d_recv.at[0, 0], z * members, t).wait_send()
 
 
-def gather_history(payload, members):
-    groups = payload.shape[0]
+def gather_history(queries, keys, values, gate, documents, members):
+    groups = gate.shape[0]
     vmem = pl.BlockSpec(memory_space=pltpu.VMEM)
     dma = pltpu.SemaphoreType.DMA
     return pl.pallas_call(
@@ -281,9 +372,12 @@
             jax.ShapeDtypeStruct((groups, BLK // 2, 128), BF16),
             jax.ShapeDtypeStruct((members, groups, KVX, 128), BF16),
         ),
-        in_specs=[vmem],
+        in_specs=[pl.BlockSpec(memory_space=pl.ANY)] * 5,
         out_specs=(vmem, vmem),
         scratch_shapes=[
+            *(pltpu.VMEM(a.shape, a.dtype) for a in (queries, keys, values, gate, documents)),
+            dma((5,)),
+            pltpu.VMEM((groups, KVX + BLK // 2, 128), BF16),
             dma,
             dma((groups,)),
             dma,
@@ -299,13 +393,13 @@
             collective_id=0, has_side_effects=True, vmem_limit_bytes=16 * 1024 * 1024
         ),
         name="gather_history",
-    )(payload)
+    )(queries, keys, values, gate, documents)
 
 
 def experts_kernel(
-    normed_ref, ow_hbm, resid_ref, ng_ref, rows_ref, cols_ref, rw_ref, wg_hbm, wu_hbm, wd_hbm,
+    normed_ref, ow_hbm, resid_hbm, ng_ref, routes_ref, rw_ref, wg_hbm, wu_hbm, wd_hbm,
     mixed_ref,
-    heads, ow, stream, out_ref, ret_ref, x, p, r_in, m_in, wg, wu, wd,
+    heads, ow, resid_ref, stream, spread_ref, out_ref, ret_ref, x, p, r_in, m_in, wg, wu, wd,
     w_sem, head_send, head_recv, a2a_send, a2a_recv, ag_send, ag_recv, relay_send, relay_recv,
     r_send, r_recv, m_send, m_recv, ret_send, ret_recv,
 ):
@@ -327,7 +421,7 @@
     loads = [
         pltpu.make_async_copy(a, b, w_sem.at[i])
         for i, (a, b) in enumerate(
-            ((ow_hbm, ow), (wg_hbm.at[0], wg), (wu_hbm.at[0], wu), (wd_hbm.at[0], wd))
+            ((ow_hbm, ow), (resid_hbm, resid_ref), (wg_hbm.at[0], wg), (wu_hbm.at[0], wu), (wd_hbm.at[0], wd))
         )
     ]
     for load in loads:
@@ -364,10 +458,30 @@
         ).start()
 
     heads[mine] = normed_ref[z, t]
-    slot_ids = lax.broadcasted_iota(jnp.int32, (experts * slots, 128), 0)
-    chosen = (slot_ids == rows_ref[0:1, :]) | (slot_ids == rows_ref[1:2, :])
-    chosen = jnp.where(chosen, 1.0, 0.0).astype(BF16)
+    rows = normed_ref.shape[3]
+    picked = jnp.concatenate(
+        [routes_ref[...].astype(F32), rw_ref[...], jnp.zeros((rows - 4, rows), F32)], axis=0
+    ).T
+    lane = lax.broadcasted_iota(jnp.int32, (rows, rows), 1)
+    below = lane < lax.broadcasted_iota(jnp.int32, (rows, rows), 0)
+    named = [jnp.where(lane.astype(F32) == picked[:, k : k + 1], 1.0, 0.0) for k in range(2)]
+    earlier = jnp.dot(
+        jnp.where(below, 1.0, 0.0).astype(BF16),
+        (named[0] + named[1]).astype(BF16),
+        preferred_element_type=F32,
+    )
+    slot_lane = lax.broadcasted_iota(jnp.int32, (rows, experts * slots), 1).astype(F32)
+    taken = [
+        slot_lane
+        == picked[:, k : k + 1] * slots + jnp.sum(named[k] * earlier, axis=1, keepdims=True)
+        for k in range(2)
+    ]
+    chosen = jnp.where(taken[0] | taken[1], 1.0, 0.0).astype(BF16)
+    spread_ref[...] = jnp.where(taken[0], picked[:, 2:3], 0.0) + jnp.where(
+        taken[1], picked[:, 3:4], 0.0
+    )
     loads[0].wait()
+    loads[1].wait()
     others = heads.at[pl.ds(0, groups * tps - 1)]
     send(others, others, head_send, head_recv, s, right).wait()
     projected = lax.dot_general(
@@ -379,7 +493,9 @@
     mean_wide = jnp.mean(widened * widened, axis=-1, keepdims=True)
     expert_input = (widened * lax.rsqrt(mean_wide + EPS) * ng_ref[...]).astype(BF16)
     out_ref[...] = (
-        jnp.dot(chosen, expert_input, preferred_element_type=F32)
+        lax.dot_general(
+            chosen, expert_input, (((0,), (0,)), ((), ())), preferred_element_type=F32
+        )
         .astype(BF16)
         .reshape(experts, slots, width)
     )
@@ -488,7 +604,7 @@
 
         @pl.when(i == 2)
         def _():
-            for load in loads[1:]:
+            for load in loads[2:]:
                 load.wait()
 
         @pl.when((i >= 2) & (i < steps + 2))
@@ -506,10 +622,7 @@
         to_side(i, some, some, relay_send.at[i], relay_recv.at[i, 0]).wait_send()
         to_side(i, some, some, r_send.at[i], r_recv.at[i, 0]).wait_send()
         to_side(i, every, every, m_send.at[i], m_recv.at[i, 0]).wait_send()
-    lanes = lax.broadcasted_iota(jnp.int32, (128, experts * slots), 1)
-    spread = jnp.where(lanes == cols_ref[:, 0:1], rw_ref[:, 0:1], 0.0) + jnp.where(
-        lanes == cols_ref[:, 1:2], rw_ref[:, 1:2], 0.0
-    )
+    spread = spread_ref[...]
     results = ret_ref[...].reshape(experts * slots, width)
     mixed = stream[...].astype(F32)
     for _ in range(3):
@@ -519,7 +632,7 @@
     mixed_ref[...] = mixed.astype(BF16)
 
 
-def at_experts(normed, out_weight, resid, norm_gain, targets, route_weights, w_gate, w_up, w_down):
+def at_experts(normed, out_weight, resid, norm_gain, routes, route_weights, w_gate, w_up, w_down):
     groups, tps = normed.shape[:2]
     rows, width = resid.shape
     hidden = w_gate.shape[2]
@@ -532,12 +645,14 @@
     return pl.pallas_call(
         experts_kernel,
         out_shape=jax.ShapeDtypeStruct((rows, width), BF16),
-        in_specs=[vmem, hbm, vmem, vmem, vmem, vmem, vmem, hbm, hbm, hbm],
+        in_specs=[vmem, hbm, hbm, vmem, vmem, vmem, hbm, hbm, hbm],
         out_specs=vmem,
         scratch_shapes=[
             pltpu.VMEM((groups * tps, 64, 128), BF16),
             pltpu.VMEM(out_weight.shape, BF16),
             pltpu.VMEM((rows, width), BF16),
+            pltpu.VMEM((rows, width), BF16),
+            pltpu.VMEM((rows, experts * slots), F32),
             pltpu.VMEM((experts, slots, width), BF16),
             pltpu.VMEM((experts, slots, width), BF16),
             pltpu.VMEM((tps, experts, slots, width), BF16),
@@ -547,7 +662,7 @@
             pltpu.VMEM((width, hidden), BF16),
             pltpu.VMEM((width, hidden), BF16),
             pltpu.VMEM((hidden, width), BF16),
-            dma((4,)),
+            dma((5,)),
             dma,
             dma,
             dma,
@@ -568,7 +683,7 @@
         ),
         name="experts",
     )(
-        normed, out_weight, resid, norm_gain.reshape(1, width), targets.T, targets, route_weights,
+        normed, out_weight, resid, norm_gain.reshape(1, width), routes.T, route_weights.T,
         w_gate, w_up, w_down,
     )
 
@@ -593,32 +708,13 @@
     heads = cum_gate.shape[1]
     sp_count = lax.axis_size("sp")
     members = sp_count // heads
-    z = lax.axis_index("sp") // members
-
-    def by_head(a):
-        return a.reshape(tokens, heads, 64).transpose(1, 0, 2)
-
-    qh = by_head(queries)
-    q_pack = jnp.concatenate([qh[:, : BLK // 2], qh[:, BLK // 2 :]], axis=-1)
-    kv = jnp.concatenate([by_head(keys), by_head(values)], axis=-1)
-    gate = cum_gate.T
-    gate0 = gate[:, :1]
-    rel = jnp.stack(pieces_of((gate0 - gate) * LOG2E), axis=1).reshape(heads, 12, 128)
-    docs = jnp.broadcast_to(documents.astype(F32).reshape(1, 4, 128), (heads, 4, 128))
-    zero_row = jnp.pad(jnp.stack(pieces_of(gate0), axis=2), ((0, 0), (0, 15), (0, 125)))
-    extra = jnp.concatenate([rel, docs, zero_row], axis=1).astype(BF16)
-    payload = jnp.concatenate([kv, extra, q_pack], axis=1)
-    q, kvx = gather_history(payload, members)
-    gain = jnp.broadcast_to(lax.dynamic_slice_in_dim(head_gain, z * 64, 64)[:, None], (64, 128))
+    q, kvx = gather_history(
+        queries, keys, values, cum_gate.T, documents.reshape(1, tokens), members
+    )
+    gain = head_gain.reshape(2, 128)
     normed = attend(q, kvx, gain)
-    flat_routes = routes.reshape(-1)
-    onehot = (flat_routes[:, None] == jnp.arange(sp_count, dtype=jnp.int32)[None, :]).astype(
-        jnp.int32
-    )
-    ranks = jnp.sum(jnp.cumsum(onehot, axis=0) * onehot, axis=1) - 1
-    targets = (flat_routes * 16 + ranks).reshape(routes.shape)
     return at_experts(
-        normed, out_weight, resid, norm_gain, targets, route_weights, w_gate, w_up, w_down
+        normed, out_weight, resid, norm_gain, routes, route_weights, w_gate, w_up, w_down
     )
 
 

time: 252 us -> 240 us (0.952)
  local copies, waits for them, and re-layouts: 13.2 us -> 7.48 us
  Pallas kernels: 236 us -> 232 us
    pallas_call x1, Pallas kernels: 177 us -> 173 us  [at_experts(): pl.pallas_call(experts_kernel, out_shape=jax.ShapeDtypeStruct((rows, widt...]
    unnamed x26 -> x15, local copies, waits for them, and re-layouts: 10.1 us -> 7.48 us
where the time goes in v2:
time: 240 us; the launch traced here: 239 us
  Pallas kernels  232 us (97%)
  local copies, waits for them, and re-layouts  7.48 us (3%)
    pallas_call x1, Pallas kernels, at_experts(): pl.pallas_call(experts_kernel, out_shape=jax.ShapeDtypeStruct((rows, widt...  173 us
    pallas_call x1, Pallas kernels, gather_history(): pl.pallas_call(gather_kernel, out_shape=(jax.ShapeDtypeStruct((groups, BL...  31.6 us
    pallas_call x1, Pallas kernels, attend(): pl.pallas_call(attention_kernel, out_shape=jax.ShapeDtypeStruct((groups,...  26.8 us
    unnamed x15, local copies, waits for them, and re-layouts  7.48 us

profile of v2, /device:TPU:1, one launch (start us, length us, event | category | flops | bytes accessed | tf_op | source)
XLA Modules:
  0.0 239.4 jit_solution(9490352221499687065)
XLA Ops:
  0.0 0.0 copy-start.1
  0.0 0.9 copy-done.1
  1.0 0.0 copy-start.2
  1.0 0.9 copy-done.2
  1.9 0.0 copy-start.3
  1.9 0.9 copy-done.3
  2.9 0.0 copy-start.4
  2.9 0.7 copy-done.4
  3.5 0.0 copy-start.5
  3.6 0.7 copy-done.5
  4.2 31.6 %gather_history.1 = (bf16[4,256,128]{2,1,0:T(8,128)(2,1)S(1)}, bf16[8,4,544,128]{3,2,1,0:T(8,128)(2,1)S(1)}) custom-call(bf16[512,256]{1,0:T(8,128)(2,1)S(1)} %copy-done.1, bf16[512,256]{1,0:T(8,128)(2,1)S(1)} %copy-done.2, bf16[512,256]{1,0:T(8,128)(2,1)S(1)} %copy-done.3, f32[4,512]{1,0:T(4,128)S(1)} %bitcast.6, s32[1,512]{1,0:T(1,128)S(1)} %bitcast.7), custom_call_target="tpu_custom_call" | custom-call | tf_op jit(solution)/shard_map/gather_history/pallas_call | solution.py:369
  35.9 0.0 copy-start.6
  35.9 0.7 copy-done.6
  36.6 26.8 %attention.1.normed_ref = bf16[4,4,64,128]{3,2,1,0:T(8,128)(2,1)S(1)} custom-call(bf16[4,256,128]{2,1,0:T(8,128)(2,1)S(1)} %get-tuple-element.7.q_hbm, bf16[8,4,544,128]{3,2,1,0:T(8,128)(2,1)S(1)} %get-tuple-element.8.kvx_hbm, f32[2,128]{1,0:T(2,128)S(1)} %bitcast.8), custom_call_target="tpu_custom_call" | custom-call | tf_op jit(solution)/shard_map/attention/pallas_call | solution.py:197
  63.3 0.0 copy-start
  63.3 0.7 copy-done
  64.0 173.4 %experts.1 = bf16[128,2048]{1,0:T(8,128)(2,1)} custom-call(bf16[4,4,64,128]{3,2,1,0:T(8,128)(2,1)} %copy-done, bf16[1024,2048]{1,0:T(8,128)(2,1)} %ow_hbm.1, bf16[128,2048]{1,0:T(8,128)(2,1)} %resid_hbm.1, f32[1,2048]{1,0:T(1,128)} %bitcast.9, s32[2,128]{1,0:T(2,128)} %bitcast.10, f32[2,128]{1,0:T(2,128)} %bitcast.11, bf16[1,2048,896]{2,1,0:T(8,128)(2,1)} %wg_hbm.1, ...), custom_call_target="tpu_custom_call" | custom-call | tf_op jit(solution)/shard_map/experts/pallas_call | solution.py:645
  237.5 1.9 copy.16
Async XLA Ops:
  0.0 0.9 copy-start.1
  1.0 0.9 copy-start.2
  1.9 0.9 copy-start.3
  2.9 0.7 copy-start.4
  3.5 0.7 copy-start.5
  35.9 0.7 copy-start.6
  63.3 0.7 copy-start

commit v3 on v2

--- a/solution.py
+++ b/solution.py
@@ -21,16 +21,17 @@
     return hi, mid, rest - mid
 
 
-def pack(queries_ref, keys_ref, values_ref, gate_ref, doc_ref, pay_ref):
+def pack(qkv_ref, small_ref, pay_ref):
     lane = lax.broadcasted_iota(jnp.int32, (BLK, 128), 1)
     half = lane[: BLK // 2]
     row_lane = lane[:1]
-    docs = doc_ref[...].astype(F32)
-    for h in range(pay_ref.shape[0]):
+    heads = pay_ref.shape[0]
+    docs = small_ref[heads : heads + 1, :]
+    for h in range(heads):
         at = slice(h // 2 * 128, h // 2 * 128 + 128)
-        k = keys_ref[:, at].astype(F32)
-        v = values_ref[:, at].astype(F32)
-        q = queries_ref[:, at].astype(F32)
+        q = qkv_ref[0:BLK, at].astype(F32)
+        k = qkv_ref[BLK : 2 * BLK, at].astype(F32)
+        v = qkv_ref[2 * BLK : 3 * BLK, at].astype(F32)
         q0, q1 = q[: BLK // 2], q[BLK // 2 :]
         if h % 2:
             k, q0 = pltpu.roll(k, 64, 1), pltpu.roll(q0, 64, 1)
@@ -38,7 +39,7 @@
             v, q1 = pltpu.roll(v, 64, 1), pltpu.roll(q1, 64, 1)
         pay_ref[h, 0:BLK, :] = jnp.where(lane < 64, k, v).astype(BF16)
         pay_ref[h, BLK + EXTRA :, :] = jnp.where(half < 64, q0, q1).astype(BF16)
-        gate = gate_ref[h : h + 1, :]
+        gate = small_ref[h : h + 1, :]
         base = gate[:, 0:1]
         rows = [
             p[:, c * 128 : (c + 1) * 128]
@@ -59,7 +60,7 @@
 
 
 def attention_kernel(
-    q_hbm, kvx_hbm, gain_ref, o_ref, q_ref, kvx_ref, kp, vt, qp, score_ref, acc, mrow, g0, q_sem, kv_sem
+    q_ref, kvx_ref, small_ref, o_ref, kp, vt, qp, score_ref, acc, mrow, g0
 ):
     members = kvx_ref.shape[0]
     groups = kvx_ref.shape[1]
@@ -71,22 +72,8 @@
     row_extra = lax.broadcasted_iota(jnp.int32, (EXTRA, 128), 0)
     is_doc = (row_extra >= 12) & (row_extra < 16)
 
-    def fetch(kb):
-        member, group = lax.rem(kb, members), kb // members
-        return pltpu.make_async_copy(
-            kvx_hbm.at[member, group], kvx_ref.at[member, group], kv_sem.at[kb]
-        )
-
-    @pl.loop(0, blocks)
-    def _(kb):
-        fetch(kb).start()
-
-    q_copy = pltpu.make_async_copy(q_hbm, q_ref, q_sem)
-    q_copy.start()
-
     def prepare(kb, counts):
         member, group = lax.rem(kb, members), kb // members
-        fetch(kb).wait()
         extra = kvx_ref[member, group, BLK : BLK + EXTRA, :].astype(F32)
         g0[kb] = jnp.sum(jnp.where(row_extra == 16, extra, 0.0))
         counts = tuple(
@@ -106,8 +93,8 @@
 
     zero = jnp.zeros((EXTRA, 128), F32)
     counts = lax.fori_loop(0, blocks, prepare, (zero, zero, zero))
-    q_copy.wait()
-    gains = jnp.broadcast_to(gain_ref[pl.ds(z // 2, 1), :], (128, 128)).T
+    gain_row = jnp.where(z < 2, small_ref[5:6, 0:128], small_ref[5:6, 128:256])
+    gains = jnp.broadcast_to(gain_row, (128, 128)).T
     gain_column = jnp.where(lax.rem(z, 2) == 0, gains[0:64], gains[64:128])
     starts = [jnp.sum(c).astype(jnp.int32) for c in counts]
 
@@ -189,19 +176,17 @@
     lax.fori_loop(0, groups, one_query_block, 0)
 
 
-def attend(q, kvx, gain):
+def attend(q, kvx, small):
     members, groups = kvx.shape[:2]
     blocks = members * groups
     vmem = pl.BlockSpec(memory_space=pltpu.VMEM)
-    hbm = pl.BlockSpec(memory_space=pl.ANY)
+    hbm = pl.BlockSpec(memory_space=pltpu.HBM)
     return pl.pallas_call(
         attention_kernel,
         out_shape=jax.ShapeDtypeStruct((groups, 4, 64, 128), BF16),
-        in_specs=[hbm, hbm, vmem],
+        in_specs=[vmem, vmem, vmem],
         out_specs=vmem,
         scratch_shapes=[
-            pltpu.VMEM(q.shape, BF16),
-            pltpu.VMEM(kvx.shape, BF16),
             pltpu.VMEM((blocks, BLK, 256), BF16),
             pltpu.VMEM((blocks, 80, BLK), BF16),
             pltpu.VMEM((BLK, 256), BF16),
@@ -209,12 +194,10 @@
             pltpu.VMEM((80, BLK), F32),
             pltpu.VMEM((1, BLK), F32),
             pltpu.SMEM((blocks,), F32),
-            pltpu.SemaphoreType.DMA,
-            pltpu.SemaphoreType.DMA((blocks,)),
         ],
         compiler_params=pltpu.CompilerParams(vmem_limit_bytes=48 * 1024 * 1024),
         name="attention",
-    )(q, kvx, gain)
+    )(q, kvx, small)
 
 
 MESH = pl.DeviceIdType.MESH
@@ -234,26 +217,11 @@
 
 
 def gather_kernel(
-    queries_hbm, keys_hbm, values_hbm, gate_hbm, doc_hbm, q_ref, kvx_ref,
-    queries_ref, keys_ref, values_ref, gate_ref, doc_ref, in_sem, pay_ref, q_send, q_recv, a_send, a_recv, y_send, y_recv,
+    qkv_ref, small_ref, q_ref, kvx_ref, pay_ref, q_send, q_recv, a_send, a_recv, y_send, y_recv,
     h_send, h_recv, d_send, d_recv,
 ):
     members, groups = kvx_ref.shape[:2]
     ring = members // 2
-    loads = [
-        pltpu.make_async_copy(a, b, in_sem.at[i])
-        for i, (a, b) in enumerate(
-            (
-                (queries_hbm, queries_ref),
-                (keys_hbm, keys_ref),
-                (values_hbm, values_ref),
-                (gate_hbm, gate_ref),
-                (doc_hbm, doc_ref),
-            )
-        )
-    ]
-    for load in loads:
-        load.start()
     s = lax.axis_index("sp")
     t = lax.axis_index("tp")
     z, j = s // members, lax.rem(s, members)
@@ -270,9 +238,7 @@
     barrier = pltpu.get_barrier_semaphore()
     for peer in peers:
         pl.semaphore_signal(barrier, 1, device_id=(peer, t), device_id_type=MESH)
-    for load in loads:
-        load.wait()
-    pack(queries_ref, keys_ref, values_ref, gate_ref, doc_ref, pay_ref)
+    pack(qkv_ref, small_ref, pay_ref)
     pl.semaphore_wait(barrier, len(peers))
 
     order = (0, 1, 3, 2)
@@ -362,8 +328,7 @@
     remote(every, every, d_send, d_recv.at[0, 0], z * members, t).wait_send()
 
 
-def gather_history(queries, keys, values, gate, documents, members):
-    groups = gate.shape[0]
+def gather_history(qkv, small, groups, members):
     vmem = pl.BlockSpec(memory_space=pltpu.VMEM)
     dma = pltpu.SemaphoreType.DMA
     return pl.pallas_call(
@@ -372,11 +337,9 @@
             jax.ShapeDtypeStruct((groups, BLK // 2, 128), BF16),
             jax.ShapeDtypeStruct((members, groups, KVX, 128), BF16),
         ),
-        in_specs=[pl.BlockSpec(memory_space=pl.ANY)] * 5,
+        in_specs=[vmem] * 2,
         out_specs=(vmem, vmem),
         scratch_shapes=[
-            *(pltpu.VMEM(a.shape, a.dtype) for a in (queries, keys, values, gate, documents)),
-            dma((5,)),
             pltpu.VMEM((groups, KVX + BLK // 2, 128), BF16),
             dma,
             dma((groups,)),
@@ -393,7 +356,7 @@
             collective_id=0, has_side_effects=True, vmem_limit_bytes=16 * 1024 * 1024
         ),
         name="gather_history",
-    )(queries, keys, values, gate, documents)
+    )(qkv, small)
 
 
 def experts_kernel(
@@ -640,7 +603,7 @@
     slots = 16
     steps = experts // GROUP
     vmem = pl.BlockSpec(memory_space=pltpu.VMEM)
-    hbm = pl.BlockSpec(memory_space=pl.ANY)
+    hbm = pl.BlockSpec(memory_space=pltpu.HBM)
     dma = pltpu.SemaphoreType.DMA
     return pl.pallas_call(
         experts_kernel,
@@ -679,7 +642,7 @@
             dma,
         ],
         compiler_params=pltpu.CompilerParams(
-            collective_id=1, has_side_effects=True, vmem_limit_bytes=60 * 1024 * 1024
+            collective_id=1, has_side_effects=True, vmem_limit_bytes=52 * 1024 * 1024
         ),
         name="experts",
     )(
@@ -708,11 +671,13 @@
     heads = cum_gate.shape[1]
     sp_count = lax.axis_size("sp")
     members = sp_count // heads
-    q, kvx = gather_history(
-        queries, keys, values, cum_gate.T, documents.reshape(1, tokens), members
-    )
-    gain = head_gain.reshape(2, 128)
-    normed = attend(q, kvx, gain)
+    qkv = jnp.concatenate([queries, keys, values], axis=0)
+    gain_row = jnp.pad(head_gain, (0, tokens - head_gain.shape[0]))
+    small = jnp.concatenate(
+        [cum_gate.T, documents.astype(F32)[None], gain_row[None]], axis=0
+    )
+    q, kvx = gather_history(qkv, small, heads, members)
+    normed = attend(q, kvx, small)
     return at_experts(
         normed, out_weight, resid, norm_gain, routes, route_weights, w_gate, w_up, w_down
     )

time: 240 us -> 234 us (0.975)
  local copies, waits for them, and re-layouts: 7.48 us -> 1.5 us
  Pallas kernels: 232 us -> 229 us
  other arithmetic: 0 us -> 2.6 us
    unnamed x15 -> x9, local copies, waits for them, and re-layouts: 7.48 us -> 0.82 us
    pallas_call x1, Pallas kernels: 26.8 us -> 23.7 us  [attend(): pl.pallas_call(attention_kernel, out_shape=jax.ShapeDtypeStruct((groups,...]
where the time goes in v3:
time: 234 us; the launch traced here: 233 us
  Pallas kernels  229 us (98%)
  other arithmetic  2.6 us (1%)
    pallas_call x1, Pallas kernels, at_experts(): pl.pallas_call(experts_kernel, out_shape=jax.ShapeDtypeStruct((rows, widt...  173 us
    pallas_call x1, Pallas kernels, gather_history(): pl.pallas_call(gather_kernel, out_shape=(jax.ShapeDtypeStruct((groups, BL...  31.6 us
    pallas_call x1, Pallas kernels, attend(): pl.pallas_call(attention_kernel, out_shape=jax.ShapeDtypeStruct((groups,...  23.7 us

profile of v3, /device:TPU:1, one launch (start us, length us, event | category | flops | bytes accessed | tf_op | source)
XLA Modules:
  0.0 232.9 jit_solution(1968261780951303184)
XLA Ops:
  0.0 0.7 convert_element_type.5
  0.7 0.7 pad.4
  1.4 0.7 pad_maximum_fusion.1.small_ref
  2.1 0.0 copy-start
  2.1 0.0 copy-start.1
  2.1 0.0 copy-start.2
  2.1 0.0 copy-start.3
  2.1 1.2 pad_maximum_fusion.qkv_ref
  3.3 31.6 %gather_history.1 = (bf16[4,256,128]{2,1,0:T(8,128)(2,1)S(1)}, bf16[8,4,544,128]{3,2,1,0:T(8,128)(2,1)S(1)}) custom-call(bf16[1536,256]{1,0:T(8,128)(2,1)S(1)} %pad_maximum_fusion.qkv_ref, f32[6,512]{1,0:T(8,128)S(1)} %pad_maximum_fusion.1.small_ref), custom_call_target="tpu_custom_call" | custom-call | tf_op jit(solution)/shard_map/gather_history/pallas_call | solution.py:334
  34.9 23.7 %attention.1.normed_ref = bf16[4,4,64,128]{3,2,1,0:T(8,128)(2,1)S(1)} custom-call(bf16[4,256,128]{2,1,0:T(8,128)(2,1)S(1)} %get-tuple-element.7.q_ref, bf16[8,4,544,128]{3,2,1,0:T(8,128)(2,1)S(1)} %get-tuple-element.8.kvx_ref, f32[6,512]{1,0:T(8,128)S(1)} %pad_maximum_fusion.1.small_ref), custom_call_target="tpu_custom_call" | custom-call | tf_op jit(solution)/shard_map/attention/pallas_call | solution.py:184
  58.6 0.0 copy-done
  58.6 0.0 copy-done.1
  58.6 0.0 copy-done.2
  58.7 0.0 copy-done.3
  58.7 173.4 %experts.1 = bf16[128,2048]{1,0:T(8,128)(2,1)S(1)} custom-call(bf16[4,4,64,128]{3,2,1,0:T(8,128)(2,1)S(1)} %attention.1.normed_ref, bf16[1024,2048]{1,0:T(8,128)(2,1)} %ow_hbm.1, bf16[128,2048]{1,0:T(8,128)(2,1)S(1)} %copy-done, f32[1,2048]{1,0:T(1,128)S(1)} %bitcast.6, s32[2,128]{1,0:T(2,128)S(1)} %bitcast.7, f32[2,128]{1,0:T(2,128)S(1)} %bitcast.8, ...), custom_call_target="tpu_custom_call" | custom-call | tf_op jit(solution)/shard_map/experts/pallas_call | solution.py:608
  232.1 0.8 copy.16
Async XLA Ops:
  2.1 56.5 %copy-start = (bf16[128,2048]{1,0:T(8,128)(2,1)S(1)}, bf16[128,2048]{1,0:T(8,128)(2,1)}, u32[]{:S(2)}) copy-start(bf16[128,2048]{1,0:T(8,128)(2,1)} %resid_hbm.1) | copy-start | bytes 1572868
  2.1 56.5 %copy-start.1 = (f32[2048]{0:T(1024)S(1)}, f32[2048]{0:T(1024)}, u32[]{:S(2)}) copy-start(f32[2048]{0:T(1024)} %param.22) | copy-start | bytes 24580
  2.1 56.5 %copy-start.2 = (s32[128,2]{0,1:T(2,128)S(1)}, s32[128,2]{0,1:T(2,128)}, u32[]{:S(2)}) copy-start(s32[128,2]{0,1:T(2,128)} %param.23) | copy-start | bytes 3076
  2.1 56.5 %copy-start.3 = (f32[128,2]{0,1:T(2,128)S(1)}, f32[128,2]{0,1:T(2,128)}, u32[]{:S(2)}) copy-start(f32[128,2]{0,1:T(2,128)} %param.24) | copy-start | bytes 3076
